TPU v7x, 32 devices: a whole 2x2x4 slice. The times are simulated.
32 devices in a mesh: sp: 16 (over z, y, x), tp: 2 (over core).
Axes of the slice: x: 2, y: 2, z: 4, core: 2. Of those that a mesh axis runs over, the one named last changes fastest.
Arguments:
- tokens: bfloat16 [4096, 4096], P('sp', 'tp'), may hold values from -480 to 480
- gain: float32 [4096], P('tp'), may hold values from 0.1 to 1.9
- q_att: bfloat16 [4096, 2048], P('sp', 'tp'), may hold values from -2.90625 to 2.90625
- k_att: bfloat16 [4096, 1024], P('sp', 'tp'), may hold values from -0.09375 to 0.09375
- v_att: bfloat16 [4096, 1024], P('sp', 'tp'), may hold values from -0.75 to 0.75
- q_ret: bfloat16 [4096, 1024], P('sp', 'tp'), may hold values from -0.09375 to 0.09375
- k_ret: bfloat16 [4096, 1024], P('sp', 'tp'), may hold values from -0.09375 to 0.09375
- v_ret: bfloat16 [4096, 1024], P('sp', 'tp'), may hold values from -0.09375 to 0.09375
- out_att: bfloat16 [2048, 4096], P('tp', 'sp'), may hold values from -0.109375 to 0.109375
- out_ret: bfloat16 [1024, 4096], P('tp', 'sp'), may hold values from -0.109375 to 0.109375
- sink: float32 [16], P('tp'), may hold values from 3 to 7
- decay_log: float32 [8, 4096], P('tp', 'sp'), may hold values from -2.125 to 0
Outputs:
- mixed: bfloat16 [4096, 4096], P(('sp', 'tp'))
- log_weight: float32 [16, 4096], P('tp', 'sp')
All inputs are finite; a program needn't handle non-finite values.
Results may differ from a plain program's by a relative error of at most 0.017.
Values may be sent and summed in bfloat16 or wider, within the bound.
A program may use at most 128 MiB of HBM per device.

v0:
```python
import jax
import jax.numpy as jnp
from jax import lax
from jax.sharding import PartitionSpec as P

D = 4096
HEAD_DIM = 128
SPAN_RADIUS = 128


def with_halo(shard, sides, width):
    for axis, dim in sides:
        peers, length = (lax.axis_size(axis), shard.shape[dim])
        up = [(i, (i + 1) % peers) for i in range(peers - 1)]
        down = [(j, i) for i, j in up]
        last = lax.slice_in_dim(shard, length - width, length, axis=dim)
        initial = lax.slice_in_dim(shard, 0, width, axis=dim)
        before = lax.ppermute(last, axis, up)
        after = lax.ppermute(initial, axis, down)
        shard = jnp.concatenate([before, shard, after], axis=dim)
    return shard


def entering(shard, axis, combine, identity, reverse):
    peers, index = (lax.axis_size(axis), lax.axis_index(axis))
    everything = jax.tree.map(
        lambda part, kind: lax.all_gather(part.astype(kind), axis),
        shard,
        (jnp.bfloat16, jnp.bfloat16),
    )
    start = jax.tree.map(
        lambda part, zero: jnp.broadcast_to(jnp.asarray(zero, part.dtype), part.shape),
        shard,
        identity,
    )

    def turn(k, before):
        at = peers - 1 - k if reverse else k
        reached = at > index if reverse else at < index
        new = combine(
            before, jax.tree.map(lambda part, own: part[at].astype(own.dtype), everything, shard)
        )
        return jax.tree.map(lambda a, b: jnp.where(reached, a, b), new, before)

    return lax.fori_loop(0, peers, turn, start)


def rotate(values, angles):
    half = values.shape[-1] // 2
    first = values[..., :half]
    second = values[..., half:]
    cosine = jnp.cos(angles)[:, None, :]
    sine = jnp.sin(angles)[:, None, :]
    return jnp.concatenate(
        [first * cosine - second * sine, second * cosine + first * sine], axis=-1
    )


def fold_with(weights, piece):
    return tuple((jnp.dot(piece, weight, preferred_element_type=jnp.float32) for weight in weights))


def chain(earlier, later):
    return (earlier[0] * later[0], later[0][:, None, None] * earlier[1] + later[1])


def shards(
    tokens, gain, q_att, k_att, v_att, q_ret, k_ret, v_ret, out_att, out_ret, sink, decay_log
):
    tok_rows = tokens.shape[0]
    att_local = sink.shape[0]
    nearby_memory = k_att.shape[1] // HEAD_DIM
    ret_local = q_ret.shape[1] // HEAD_DIM
    group = att_local // nearby_memory
    total_rows = tok_rows * lax.axis_size("sp")
    offset = lax.axis_index("sp") * tok_rows
    highest = lax.Precision.HIGHEST
    widened = tokens.astype(jnp.float32)
    squares = lax.psum(jnp.sum(widened * widened, axis=1), "tp")
    inverse = lax.rsqrt(squares / D + 1e-06)[:, None]
    scaled = (widened * gain).astype(jnp.bfloat16)
    wide_qa, wide_ka, wide_va, wide_qr, wide_kr, wide_vr = (
        lax.all_gather(q_att, "sp", axis=0, tiled=True),
        lax.all_gather(k_att, "sp", axis=0, tiled=True),
        lax.all_gather(v_att, "sp", axis=0, tiled=True),
        lax.all_gather(q_ret, "sp", axis=0, tiled=True),
        lax.all_gather(k_ret, "sp", axis=0, tiled=True),
        lax.all_gather(v_ret, "sp", axis=0, tiled=True),
    )
    every_weight = (wide_qa, wide_ka, wide_va, wide_qr, wide_kr, wide_vr)
    proj_qa, proj_ka, proj_va, proj_qr, proj_kr, proj_vr = fold_with(
        every_weight, lax.all_gather(scaled, "tp", axis=1, tiled=True)
    )
    positions = (offset + jnp.arange(tok_rows, dtype=jnp.int32)).astype(jnp.float32)
    freqs = 10000.0 ** (-jnp.arange(0, HEAD_DIM, 2).astype(jnp.float32) / HEAD_DIM)
    angles = positions[:, None] * freqs[None, :]
    att_query = rotate((proj_qa * inverse).reshape(tok_rows, att_local, HEAD_DIM), angles).astype(
        jnp.bfloat16
    )
    att_key = rotate((proj_ka * inverse).reshape(tok_rows, nearby_memory, HEAD_DIM), angles).astype(
        jnp.bfloat16
    )
    att_value = (proj_va * inverse).astype(jnp.bfloat16).reshape(tok_rows, nearby_memory, HEAD_DIM)
    stacked = jnp.stack([att_key, att_value])
    widened_pair = with_halo(stacked, (("sp", 1),), SPAN_RADIUS)
    block_rows = min(tok_rows, 512)
    sink_logit = sink.reshape(nearby_memory, group)
    grouped_query = att_query.reshape(tok_rows, nearby_memory, group, HEAD_DIM)

    def attend_block(index):
        begin = index * block_rows
        block_keys = widened_pair[0]
        block_values = widened_pair[1]
        scores = jnp.einsum(
            "qhgd,khd->hgqk", grouped_query, block_keys, preferred_element_type=jnp.float32
        ) * HEAD_DIM ** (-0.5)
        query_pos = offset + begin + jnp.arange(block_rows, dtype=jnp.int32)
        key_pos = (
            offset + begin - SPAN_RADIUS + jnp.arange(block_rows + 2 * SPAN_RADIUS, dtype=jnp.int32)
        )
        spacing = key_pos[None, :] - query_pos[:, None]
        valid = (
            (jnp.abs(spacing) <= SPAN_RADIUS)
            & (key_pos >= 0)[None, :]
            & (key_pos < total_rows)[None, :]
        )
        masked = jnp.where(valid, scores, -jnp.inf)
        top = jnp.maximum(jnp.max(masked, axis=-1), sink_logit[:, :, None])
        expo = jnp.exp(masked - top[..., None])
        total = jnp.sum(expo, axis=-1) + jnp.exp(sink_logit[:, :, None] - top)
        logs = top + jnp.log(total)
        probs = (expo / total[..., None]).astype(jnp.bfloat16)
        result = jnp.einsum(
            "hgqk,khd->qhgd", probs, block_values, preferred_element_type=jnp.float32
        ).astype(jnp.bfloat16)
        return (
            result.reshape(block_rows, att_local * HEAD_DIM),
            logs.reshape(att_local, block_rows),
        )

    att_blocks, log_blocks = lax.map(
        attend_block, jnp.arange(tok_rows // block_rows, dtype=jnp.int32)
    )
    att_out = att_blocks.reshape(tok_rows, att_local * HEAD_DIM)
    log_weight = jnp.moveaxis(log_blocks, 0, 1).reshape(att_local, tok_rows)
    ret_query = (proj_qr * inverse).astype(jnp.bfloat16).reshape(tok_rows, ret_local, HEAD_DIM)
    ret_key = (
        (proj_kr * (inverse * HEAD_DIM ** (-0.5)))
        .astype(jnp.bfloat16)
        .reshape(tok_rows, ret_local, HEAD_DIM)
    )
    ret_value = (proj_vr * inverse).astype(jnp.bfloat16).reshape(tok_rows, ret_local, HEAD_DIM)
    cumul = jnp.cumsum(decay_log, axis=1)
    last = cumul[:, -1]
    query_f = ret_query.astype(jnp.float32)
    key_f = ret_key.astype(jnp.float32)
    value_f = ret_value.astype(jnp.float32)
    ret_scores = jnp.einsum("qhd,khd->hqk", ret_query, ret_key, preferred_element_type=jnp.float32)
    decay_weights = jnp.exp(-jnp.abs(cumul[:, :, None] - cumul[:, None, :]))
    inner = jnp.einsum("hqk,khd->qhd", ret_scores * decay_weights, value_f, precision=highest)
    trailing = jnp.exp(last[:, None] - cumul)
    leading = jnp.exp(cumul)
    forward_state = jnp.einsum("hk,khd,khe->hde", trailing, key_f, value_f, precision=highest)
    backward_state = jnp.einsum("hk,khd,khe->hde", leading, key_f, value_f, precision=highest)
    decay_total = jnp.exp(last)
    identity = (jnp.ones_like(decay_total), jnp.zeros_like(forward_state))
    from_before = entering((decay_total, forward_state), "sp", chain, identity, False)[1]
    from_after = entering((decay_total, backward_state), "sp", chain, identity, True)[1]
    carried = leading.T[:, :, None] * jnp.einsum(
        "qhd,hde->qhe", query_f, from_before, precision=highest
    )
    carried = carried + trailing.T[:, :, None] * jnp.einsum(
        "qhd,hde->qhe", query_f, from_after, precision=highest
    )
    blended_output = inner + carried
    middle_point = blended_output - jnp.mean(blended_output, axis=-1, keepdims=True)
    normed = middle_point * lax.rsqrt(
        jnp.mean(middle_point * middle_point, axis=-1, keepdims=True) + 1e-06
    )
    ret_out = normed.astype(jnp.bfloat16).reshape(tok_rows, ret_local * HEAD_DIM)
    wide_out_att, wide_out_ret = (
        lax.all_gather(out_att, "sp", axis=1, tiled=True),
        lax.all_gather(out_ret, "sp", axis=1, tiled=True),
    )
    mixed = lax.psum_scatter(
        (
            jnp.dot(att_out, wide_out_att, preferred_element_type=jnp.float32)
            + jnp.dot(ret_out, wide_out_ret, preferred_element_type=jnp.float32)
        ).astype(jnp.bfloat16),
        "tp",
        scatter_dimension=0,
        tiled=True,
    )
    return (mixed, log_weight)


def solution(mesh):
    return jax.shard_map(
        shards,
        mesh=mesh,
        in_specs=(
            P("sp", "tp"),
            P("tp"),
            P("sp", "tp"),
            P("sp", "tp"),
            P("sp", "tp"),
            P("sp", "tp"),
            P("sp", "tp"),
            P("sp", "tp"),
            P("tp", "sp"),
            P("tp", "sp"),
            P("tp"),
            P("tp", "sp"),
        ),
        out_specs=(P(("sp", "tp"), None), P("tp", "sp")),
        check_vma=False,
    )
```

profile of v0, /device:TPU:0, one launch (start us, length us, event | category | flops | bytes accessed | tf_op | source)
XLA Modules:
  0.0 895.8 jit_solution(7735527587921231865)
XLA Ops:
  17.5 5.9 all-gather.15.cloned.1.call-done
  23.4 79.6 %all-gather.29.cloned.1.call-done = bf16[4096,512]{1,0:T(8,128)(2,1)} async-done(((bf16[256,512]{1,0:T(8,128)(2,1)}), bf16[4096,512]{1,0:T(8,128)(2,1)}) %all-gather.29.cloned.1.call-update) | async-done | bytes 4194320 | tf_op jit(solution)/shard_map/all_gather | solution.py:87
  103.0 4.1 fusion.17
  107.2 72.8 %all-gather.25.cloned.1.call-done = bf16[4096,512]{1,0:T(8,128)(2,1)} async-done(((bf16[256,512]{1,0:T(8,128)(2,1)}), bf16[4096,512]{1,0:T(8,128)(2,1)}) %all-gather.25.cloned.1.call-update) | async-done | bytes 4194320 | tf_op jit(solution)/shard_map/all_gather | solution.py:88
  180.0 4.1 fusion.19
  190.1 39.8 %all-reduce = bf16[64]{0:T(256)(128)(2,1)S(1)} all-reduce(bf16[64]{0:T(256)(128)(2,1)S(1)} %dynamic-update-slice), channel_id=2, replica_groups=mesh['sp'=16,'tp'=2] {'sp'}, use_global_device_ids=true, to_apply=%add | all-reduce | flops 64 | bytes 256
  231.4 25.6 %all-gather.17.cloned.1.call-done = bf16[4096,512]{1,0:T(8,128)(2,1)} async-done(((bf16[256,512]{1,0:T(8,128)(2,1)}), bf16[4096,512]{1,0:T(8,128)(2,1)}) %all-gather.17.cloned.1.call-update) | async-done | bytes 4194320 | tf_op jit(solution)/shard_map/all_gather | solution.py:84
  257.1 4.1 convolution_multiply_fusion.6
  261.7 72.2 %all-gather.19.cloned.1.call-done = bf16[4096,512]{1,0:T(8,128)(2,1)} async-done(((bf16[256,512]{1,0:T(8,128)(2,1)}), bf16[4096,512]{1,0:T(8,128)(2,1)}) %all-gather.19.cloned.1.call-update) | async-done | bytes 4194320 | tf_op jit(solution)/shard_map/all_gather | solution.py:85
  333.9 4.1 fusion.14
  339.2 3.4 collective-permute-start
  343.9 70.2 %all-gather.27.cloned.1.call-done = bf16[4096,512]{1,0:T(8,128)(2,1)} async-done(((bf16[256,512]{1,0:T(8,128)(2,1)}), bf16[4096,512]{1,0:T(8,128)(2,1)}) %all-gather.27.cloned.1.call-update) | async-done | bytes 4194320 | tf_op jit(solution)/shard_map/all_gather | solution.py:86
  414.0 4.1 fusion.18
  420.6 55.2 %all-gather.35.cloned.1.call-done = bf16[64,128,128]{2,1,0:T(8,128)(2,1)} async-done(((bf16[4,128,128]{2,1,0:T(8,128)(2,1)}), bf16[64,128,128]{2,1,0:T(8,128)(2,1)}) %all-gather.35.cloned.1.call-update) | async-done | bytes 2097168 | tf_op jit(solution)/shard_map/all_gather | solution.py:27
  475.8 27.7 %while.36 = (s32[]{:T(128)}, f32[4,128,128]{2,1,0:T(8,128)S(1)}, s32[]{:T(128)}, bf16[16,4]{1,0:T(8,128)(2,1)}, bf16[16,4,128,128]{3,2,1,0:T(8,128)(2,1)}, /*index=5*/s32[]{:T(128)}, s32[]{:T(128)}, s32[]{:T(128)}, s32[]{:T(128)}) while((s32[]{:T(128)}, f32[4,128,128]{2,1,0:T(8,128)S(1)}, s32[]{:T(128)}, bf16[16,4]{1,0:T(8,128)(2,1)}, ...), condition=%wide.region_9.10_spmd.clone, body=%wide.region_8.9_spmd.clone.sunk | while | flops 327692 | bytes 655567 | solution.py:45
  503.5 34.4 %all-gather.33.cloned.1.call-done = bf16[64,128,128]{2,1,0:T(8,128)(2,1)} async-done(((bf16[4,128,128]{2,1,0:T(8,128)(2,1)}), bf16[64,128,128]{2,1,0:T(8,128)(2,1)}) %all-gather.33.cloned.1.call-update) | async-done | bytes 2097168 | tf_op jit(solution)/shard_map/all_gather | solution.py:27
  537.9 27.5 %while.35 = (s32[]{:T(128)}, f32[4,128,128]{2,1,0:T(8,128)S(1)}, s32[]{:T(128)}, bf16[16,4]{1,0:T(8,128)(2,1)}, bf16[16,4,128,128]{3,2,1,0:T(8,128)(2,1)}, /*index=5*/s32[]{:T(128)}, s32[]{:T(128)}) while((s32[]{:T(128)}, f32[4,128,128]{2,1,0:T(8,128)S(1)}, s32[]{:T(128)}, bf16[16,4]{1,0:T(8,128)(2,1)}, ...), condition=%wide.region_7.8_spmd.clone, body=%wide.region_6.7_spmd.clone.sunk | while | flops 327688 | bytes 655505 | solution.py:45
  567.2 84.6 %all-gather.21.cloned.1.call-done = bf16[4096,1024]{1,0:T(8,128)(2,1)} async-done(((bf16[256,1024]{1,0:T(8,128)(2,1)}), bf16[4096,1024]{1,0:T(8,128)(2,1)}) %all-gather.21.cloned.1.call-update) | async-done | bytes 8388624 | tf_op jit(solution)/shard_map/all_gather | solution.py:83
  651.8 6.3 fusion.8
  662.4 124.7 %all-gather.23.cloned.1.call-done = bf16[1024,4096]{1,0:T(8,128)(2,1)} async-done(((bf16[1024,256]{1,0:T(8,128)(2,1)}), bf16[1024,4096]{1,0:T(8,128)(2,1)}) %all-gather.23.cloned.1.call-update) | async-done | bytes 8388624 | tf_op jit(solution)/shard_map/all_gather | solution.py:182
  787.1 7.8 fusion.51
  794.8 80.0 %all-gather.31.cloned.1.call-done = bf16[512,4096]{1,0:T(8,128)(2,1)} async-done(((bf16[512,256]{1,0:T(8,128)(2,1)}), bf16[512,4096]{1,0:T(8,128)(2,1)}) %all-gather.31.cloned.1.call-update) | async-done | bytes 4194320 | tf_op jit(solution)/shard_map/all_gather | solution.py:183
  874.8 6.1 fusion.2
  881.6 7.4 reduce-scatter.2.cloned.1.call-done
  (170 shorter events, 83.6 us)
Async XLA Ops:
  7.2 5.9 copy-start.3
  7.2 16.3 %all-gather.15.cloned.1.call-start = ((), (), s32[]{:S(2)}) async-start(), calls=%async_computation.1 | async-start | bytes 3145728 | tf_op jit(solution)/shard_map/all_gather | solution.py:92
  9.7 93.3 %all-gather.29.cloned.1.call-start = ((), (), s32[]{:S(2)}) async-start(), calls=%async_computation.8 | async-start | bytes 4456448 | tf_op jit(solution)/shard_map/all_gather | solution.py:87
  10.5 169.5 %all-gather.25.cloned.1.call-start = ((), (), s32[]{:S(2)}) async-start(), calls=%async_computation.6 | async-start | bytes 4456448 | tf_op jit(solution)/shard_map/all_gather | solution.py:88
  11.2 245.8 %all-gather.17.cloned.1.call-start = ((), (), s32[]{:S(2)}) async-start(), calls=%async_computation.2 | async-start | bytes 4456448 | tf_op jit(solution)/shard_map/all_gather | solution.py:84
  11.8 322.1 %all-gather.19.cloned.1.call-start = ((), (), s32[]{:S(2)}) async-start(), calls=%async_computation.3 | async-start | bytes 4456448 | tf_op jit(solution)/shard_map/all_gather | solution.py:85
  12.4 401.6 %all-gather.27.cloned.1.call-start = ((), (), s32[]{:S(2)}) async-start(), calls=%async_computation.7 | async-start | bytes 4456448 | tf_op jit(solution)/shard_map/all_gather | solution.py:86
  13.0 462.8 %all-gather.35.cloned.1.call-start = ((), (), s32[]{:S(2)}) async-start(), calls=%async_computation.12 | async-start | bytes 2228224 | tf_op jit(solution)/shard_map/all_gather | solution.py:27
  17.5 316.5 %copy-start.6 = (f32[256]{0:T(256)}, f32[256]{0:T(256)S(1)}, u32[]{:S(2)}) copy-start(f32[256]{0:T(256)S(1)} %get-tuple-element.322) | copy-start | bytes 3076
  107.2 78.0 %copy-start.1 = (bf16[256,512]{0,1:T(8,128)(2,1)}, bf16[256,512]{0,1:T(8,128)(2,1)S(1)}, u32[]{:S(2)}) copy-start(bf16[256,512]{0,1:T(8,128)(2,1)S(1)} %copy.80) | copy-start | bytes 786436
  180.0 8.5 copy-start.4
  180.0 8.6 copy-start.8
  185.2 352.7 %all-gather.33.cloned.1.call-start = ((), (), s32[]{:S(2)}) async-start(), calls=%async_computation.11 | async-start | bytes 2228224 | tf_op jit(solution)/shard_map/all_gather | solution.py:27
  186.3 465.5 %all-gather.21.cloned.1.call-start = ((), (), s32[]{:S(2)}) async-start(), calls=%async_computation.4 | async-start | bytes 8912896 | tf_op jit(solution)/shard_map/all_gather | solution.py:83
  187.1 600.0 %all-gather.23.cloned.1.call-start = ((), (), s32[]{:S(2)}) async-start(), calls=%async_computation.5 | async-start | bytes 8912896 | tf_op jit(solution)/shard_map/all_gather | solution.py:182
  187.6 687.1 %all-gather.31.cloned.1.call-start = ((), (), s32[]{:S(2)}) async-start(), calls=%async_computation.9 | async-start | bytes 4456448 | tf_op jit(solution)/shard_map/all_gather | solution.py:183
  188.4 700.6 %reduce-scatter.2.cloned.1.call-start = ((), (), s32[]{:S(2)}) async-start(), calls=%async_computation.10 | async-start | bytes 3145728 | tf_op jit(solution)/shard_map/reduce_scatter | solution.py:185
  338.4 79.7 %copy-start.2 = (bf16[256,512]{0,1:T(8,128)(2,1)S(1)}, bf16[256,512]{0,1:T(8,128)(2,1)}, u32[]{:S(2)}) copy-start(bf16[256,512]{0,1:T(8,128)(2,1)} %copy-done.1) | copy-start | bytes 786436
  339.2 80.2 %collective-permute-start = (bf16[2,128,4,128]{3,1,2,0:T(8,128)(2,1)}, bf16[2,128,4,128]{3,1,2,0:T(8,128)(2,1)S(1)}, u32[]{:S(2)}, u32[]{:S(2)}) collective-permute-start(bf16[2,128,4,128]{3,1,2,0:T(8,128)(2,1)} %get-tuple-element.313), channel_id=1, source_target_pairs={{0,2},{2,4},{4,6},{6,8},{8,10},{10,12},{12,14},{14,16},{16,18},{18... | collective-permute-start | bytes 786440 | tf_op jit(solution)/shard_map/ppermute | solution.py:18
  342.6 76.9 %collective-permute-start.1 = (bf16[2,128,4,128]{3,1,2,0:T(8,128)(2,1)S(1)}, bf16[2,128,4,128]{3,1,2,0:T(8,128)(2,1)}, u32[]{:S(2)}, u32[]{:S(2)}) collective-permute-start(bf16[2,128,4,128]{3,1,2,0:T(8,128)(2,1)S(1)} %get-tuple-element.314), channel_id=1, source_target_pairs={{2,0},{4,2},{6,4},{8,6},{10,8},{12,10},{14,12},{16,14},{18,16},{20... | collective-permute-start | bytes 786440 | tf_op jit(solution)/shard_map/ppermute | solution.py:19
  475.8 90.5 %copy-start = (f32[4,256,256]{2,1,0:T(8,128)S(1)}, f32[4,256,256]{2,1,0:T(8,128)}, u32[]{:S(2)}) copy-start(f32[4,256,256]{2,1,0:T(8,128)} %convolution_multiply_fusion) | copy-start | bytes 3145732
  565.4 86.4 %copy-start.7 = (f32[256]{0:T(256)S(1)}, f32[256]{0:T(256)}, u32[]{:S(2)}) copy-start(f32[256]{0:T(256)} %copy-done.6) | copy-start | bytes 3076
  874.8 6.1 copy-start.5
Sparse Core Ops, SparseCore 0:
  10.1 13.2 all-gather.14
  26.2 76.7 all-gather.28
  105.8 74.1 all-gather.24
  182.6 74.4 all-gather.16
  259.7 74.1 all-gather.18
  336.5 77.4 all-gather.26
  416.8 58.9 all-gather.34
  478.6 59.2 all-gather.32
  540.7 111.0 all-gather.20
  654.4 132.6 all-gather.22
  789.8 84.9 all-gather.30
  881.0 7.9 reduce-scatter.1
where the time goes:
time: 897 us; the launch traced here: 896 us
  waiting for transfers between devices  717 us (80%)
  other arithmetic  63.1 us (7%)
  matrix products  47.8 us (5%)
  blocking collectives  42.4 us (5%)
  between operations  15.3 us (2%)
    all_gather x1, waiting for transfers between devices, shards(): lax.all_gather(out_att, 'sp', axis=1, tiled=True)  125 us
    all_gather x2, waiting for transfers between devices, entering(): lax.all_gather(part.astype(kind), axis)  89.6 us
    all_gather x1, waiting for transfers between devices, shards(): lax.all_gather(q_att, 'sp', axis=0, tiled=True)  84.6 us
    all_gather x1, waiting for transfers between devices, shards(): lax.all_gather(out_ret, 'sp', axis=1, tiled=True)  80 us
    all_gather x1, waiting for transfers between devices, shards(): lax.all_gather(k_ret, 'sp', axis=0, tiled=True)  79.6 us
    all_gather x1, waiting for transfers between devices, shards(): lax.all_gather(v_ret, 'sp', axis=0, tiled=True)  72.8 us
    all_gather x1, waiting for transfers between devices, shards(): lax.all_gather(v_att, 'sp', axis=0, tiled=True)  72.2 us
    all_gather x1, waiting for transfers between devices, shards(): lax.all_gather(q_ret, 'sp', axis=0, tiled=True)  70.2 us
  transfers between devices with their start and end apart: 14, of which 12 were waited for; matrix products, arithmetic and copies ran while one was open for 12% of the time, Pallas kernels for 0%

commit v1 on v0

--- a/solution.py
+++ b/solution.py
@@ -180,7 +180,7 @@
     ret_out = normed.astype(jnp.bfloat16).reshape(tok_rows, ret_local * HEAD_DIM)
     wide_out_att, wide_out_ret = (
         lax.all_gather(out_att, "sp", axis=1, tiled=True),
-        lax.all_gather(out_ret, "sp", axis=1, tiled=True),
+        jnp.concatenate(lax.all_gather(out_ret, "sp"), axis=1),
     )
     mixed = lax.psum_scatter(
         (

time: 897 us -> 889 us (level)
  waiting for transfers between devices: 717 us -> 706 us
    all_gather x1, waiting for transfers between devices: 80 us -> 69.9 us  [shards(): lax.all_gather(out_ret, 'sp')]
where the time goes in v1:
time: 889 us; the launch traced here: 887 us
  waiting for transfers between devices  706 us (79%)
  other arithmetic  62.1 us (7%)
  matrix products  45 us (5%)
  blocking collectives  42.4 us (5%)
  between operations  15.3 us (2%)
  local copies, waits for them, and re-layouts  9.69 us (1%)
    all_gather x1, waiting for transfers between devices, shards(): lax.all_gather(out_att, 'sp', axis=1, tiled=True)  125 us
    all_gather x2, waiting for transfers between devices, entering(): lax.all_gather(part.astype(kind), axis)  89.2 us
    all_gather x1, waiting for transfers between devices, shards(): lax.all_gather(q_att, 'sp', axis=0, tiled=True)  82.9 us
    all_gather x1, waiting for transfers between devices, shards(): lax.all_gather(k_ret, 'sp', axis=0, tiled=True)  79.6 us
    all_gather x1, waiting for transfers between devices, shards(): lax.all_gather(v_ret, 'sp', axis=0, tiled=True)  72.8 us
    all_gather x1, waiting for transfers between devices, shards(): lax.all_gather(v_att, 'sp', axis=0, tiled=True)  72.2 us
    all_gather x1, waiting for transfers between devices, shards(): lax.all_gather(q_ret, 'sp', axis=0, tiled=True)  70.6 us
    all_gather x1, waiting for transfers between devices, shards(): lax.all_gather(out_ret, 'sp')  69.9 us
  transfers between devices with their start and end apart: 14, of which 12 were waited for; matrix products, arithmetic and copies ran while one was open for 12% of the time, Pallas kernels for 0%

profile of v1, /device:TPU:0, one launch (start us, length us, event | category | flops | bytes accessed | tf_op | source)
XLA Modules:
  0.0 886.7 jit_solution(8374671692666924115)
XLA Ops:
  18.3 5.2 all-gather.16.cloned.1.call-done
  23.4 79.6 %all-gather.30.cloned.1.call-done = bf16[4096,512]{1,0:T(8,128)(2,1)} async-done(((bf16[256,512]{1,0:T(8,128)(2,1)}), bf16[4096,512]{1,0:T(8,128)(2,1)}) %all-gather.30.cloned.1.call-update) | async-done | bytes 4194320 | tf_op jit(solution)/shard_map/all_gather | solution.py:87
  103.0 4.1 fusion.17
  107.2 72.8 %all-gather.26.cloned.1.call-done = bf16[4096,512]{1,0:T(8,128)(2,1)} async-done(((bf16[256,512]{1,0:T(8,128)(2,1)}), bf16[4096,512]{1,0:T(8,128)(2,1)}) %all-gather.26.cloned.1.call-update) | async-done | bytes 4194320 | tf_op jit(solution)/shard_map/all_gather | solution.py:88
  180.0 3.5 fusion.19
  188.8 39.8 %all-reduce = bf16[64]{0:T(256)(128)(2,1)S(1)} all-reduce(bf16[64]{0:T(256)(128)(2,1)S(1)} %dynamic-update-slice), channel_id=2, replica_groups=mesh['sp'=16,'tp'=2] {'sp'}, use_global_device_ids=true, to_apply=%add | all-reduce | flops 64 | bytes 256
  230.2 26.9 %all-gather.18.cloned.1.call-done = bf16[4096,512]{1,0:T(8,128)(2,1)} async-done(((bf16[256,512]{1,0:T(8,128)(2,1)}), bf16[4096,512]{1,0:T(8,128)(2,1)}) %all-gather.18.cloned.1.call-update) | async-done | bytes 4194320 | tf_op jit(solution)/shard_map/all_gather | solution.py:84
  257.1 4.1 convolution_multiply_fusion.6
  261.7 72.2 %all-gather.20.cloned.1.call-done = bf16[4096,512]{1,0:T(8,128)(2,1)} async-done(((bf16[256,512]{1,0:T(8,128)(2,1)}), bf16[4096,512]{1,0:T(8,128)(2,1)}) %all-gather.20.cloned.1.call-update) | async-done | bytes 4194320 | tf_op jit(solution)/shard_map/all_gather | solution.py:85
  333.9 4.1 fusion.14
  338.5 3.4 collective-permute-start
  343.1 69.9 %all-gather.36.cloned.1.call-done = bf16[8192,256]{1,0:T(8,128)(2,1)} async-done(((bf16[512,256]{1,0:T(8,128)(2,1)}), bf16[8192,256]{1,0:T(8,128)(2,1)}) %all-gather.36.cloned.1.call-update) | async-done | bytes 4194320 | tf_op jit(solution)/shard_map/all_gather | solution.py:183
  413.0 6.4 copy.91
  419.4 70.6 %all-gather.28.cloned.1.call-done = bf16[4096,512]{1,0:T(8,128)(2,1)} async-done(((bf16[256,512]{1,0:T(8,128)(2,1)}), bf16[4096,512]{1,0:T(8,128)(2,1)}) %all-gather.28.cloned.1.call-update) | async-done | bytes 4194320 | tf_op jit(solution)/shard_map/all_gather | solution.py:86
  490.0 4.1 fusion.18
  495.6 56.2 %all-gather.34.cloned.1.call-done = bf16[64,128,128]{2,1,0:T(8,128)(2,1)} async-done(((bf16[4,128,128]{2,1,0:T(8,128)(2,1)}), bf16[64,128,128]{2,1,0:T(8,128)(2,1)}) %all-gather.34.cloned.1.call-update) | async-done | bytes 2097168 | tf_op jit(solution)/shard_map/all_gather | solution.py:27
  551.8 27.7 %while.36 = (s32[]{:T(128)}, f32[4,128,128]{2,1,0:T(8,128)S(1)}, s32[]{:T(128)}, bf16[16,4]{1,0:T(8,128)(2,1)}, bf16[16,4,128,128]{3,2,1,0:T(8,128)(2,1)}, /*index=5*/s32[]{:T(128)}, s32[]{:T(128)}, s32[]{:T(128)}, s32[]{:T(128)}) while((s32[]{:T(128)}, f32[4,128,128]{2,1,0:T(8,128)S(1)}, s32[]{:T(128)}, bf16[16,4]{1,0:T(8,128)(2,1)}, ...), condition=%wide.region_9.10_spmd.clone, body=%wide.region_8.9_spmd.clone.sunk | while | flops 327692 | bytes 655567 | solution.py:45
  580.9 32.9 %all-gather.32.cloned.1.call-done = bf16[64,128,128]{2,1,0:T(8,128)(2,1)} async-done(((bf16[4,128,128]{2,1,0:T(8,128)(2,1)}), bf16[64,128,128]{2,1,0:T(8,128)(2,1)}) %all-gather.32.cloned.1.call-update) | async-done | bytes 2097168 | tf_op jit(solution)/shard_map/all_gather | solution.py:27
  613.8 27.7 %while.35 = (s32[]{:T(128)}, f32[4,128,128]{2,1,0:T(8,128)S(1)}, s32[]{:T(128)}, bf16[16,4]{1,0:T(8,128)(2,1)}, bf16[16,4,128,128]{3,2,1,0:T(8,128)(2,1)}, /*index=5*/s32[]{:T(128)}, s32[]{:T(128)}) while((s32[]{:T(128)}, f32[4,128,128]{2,1,0:T(8,128)S(1)}, s32[]{:T(128)}, bf16[16,4]{1,0:T(8,128)(2,1)}, ...), condition=%wide.region_7.8_spmd.clone, body=%wide.region_6.7_spmd.clone.sunk | while | flops 327688 | bytes 655505 | solution.py:45
  644.7 82.9 %all-gather.22.cloned.1.call-done = bf16[4096,1024]{1,0:T(8,128)(2,1)} async-done(((bf16[256,1024]{1,0:T(8,128)(2,1)}), bf16[4096,1024]{1,0:T(8,128)(2,1)}) %all-gather.22.cloned.1.call-update) | async-done | bytes 8388624 | tf_op jit(solution)/shard_map/all_gather | solution.py:83
  727.6 6.3 fusion.8
  738.1 124.8 %all-gather.24.cloned.1.call-done = bf16[1024,4096]{1,0:T(8,128)(2,1)} async-done(((bf16[1024,256]{1,0:T(8,128)(2,1)}), bf16[1024,4096]{1,0:T(8,128)(2,1)}) %all-gather.24.cloned.1.call-update) | async-done | bytes 8388624 | tf_op jit(solution)/shard_map/all_gather | solution.py:182
  863.0 6.0 fusion.51
  872.5 7.4 reduce-scatter.2.cloned.1.call-done
  (177 shorter events, 87.5 us)
Async XLA Ops:
  7.2 6.6 copy-start.4
  7.2 16.3 %all-gather.16.cloned.1.call-start = ((), (), s32[]{:S(2)}) async-start(), calls=%async_computation.1 | async-start | bytes 3145728 | tf_op jit(solution)/shard_map/all_gather | solution.py:92
  9.7 93.3 %all-gather.30.cloned.1.call-start = ((), (), s32[]{:S(2)}) async-start(), calls=%async_computation.8 | async-start | bytes 4456448 | tf_op jit(solution)/shard_map/all_gather | solution.py:87
  10.5 169.5 %all-gather.26.cloned.1.call-start = ((), (), s32[]{:S(2)}) async-start(), calls=%async_computation.6 | async-start | bytes 4456448 | tf_op jit(solution)/shard_map/all_gather | solution.py:88
  11.2 245.8 %all-gather.18.cloned.1.call-start = ((), (), s32[]{:S(2)}) async-start(), calls=%async_computation.2 | async-start | bytes 4456448 | tf_op jit(solution)/shard_map/all_gather | solution.py:84
  11.8 322.1 %all-gather.20.cloned.1.call-start = ((), (), s32[]{:S(2)}) async-start(), calls=%async_computation.3 | async-start | bytes 4456448 | tf_op jit(solution)/shard_map/all_gather | solution.py:85
  12.4 400.6 %all-gather.36.cloned.1.call-start = ((), (), s32[]{:S(2)}) async-start(), calls=%async_computation.12 | async-start | bytes 4456448 | tf_op jit(solution)/shard_map/all_gather | solution.py:183
  13.0 477.0 %all-gather.28.cloned.1.call-start = ((), (), s32[]{:S(2)}) async-start(), calls=%async_computation.7 | async-start | bytes 4456448 | tf_op jit(solution)/shard_map/all_gather | solution.py:86
  13.7 538.1 %all-gather.34.cloned.1.call-start = ((), (), s32[]{:S(2)}) async-start(), calls=%async_computation.11 | async-start | bytes 2228224 | tf_op jit(solution)/shard_map/all_gather | solution.py:27
  18.2 315.7 %copy-start.7 = (f32[256]{0:T(256)}, f32[256]{0:T(256)S(1)}, u32[]{:S(2)}) copy-start(f32[256]{0:T(256)S(1)} %get-tuple-element.322) | copy-start | bytes 3076
  23.4 156.6 %copy-start.10 = (bf16[256,4096]{1,0:T(8,128)(2,1)S(1)}, bf16[256,4096]{1,0:T(8,128)(2,1)}, u32[]{:S(2)}) copy-start(bf16[256,4096]{1,0:T(8,128)(2,1)} %all-gather.16.cloned.1.call-done) | copy-start | bytes 6291460
  180.0 7.3 copy-start.11
  180.0 49.3 %copy-start.5 = (f32[8]{0:T(128)S(1)}, f32[8]{0:T(128)}, u32[]{:S(2)}) copy-start(f32[8]{0:T(128)} %param.26) | copy-start | bytes 100
  183.5 3.6 copy-start.3
  184.6 429.1 %all-gather.32.cloned.1.call-start = ((), (), s32[]{:S(2)}) async-start(), calls=%async_computation.10 | async-start | bytes 2228224 | tf_op jit(solution)/shard_map/all_gather | solution.py:27
  185.8 541.8 %all-gather.22.cloned.1.call-start = ((), (), s32[]{:S(2)}) async-start(), calls=%async_computation.4 | async-start | bytes 8912896 | tf_op jit(solution)/shard_map/all_gather | solution.py:83
  186.4 676.6 %all-gather.24.cloned.1.call-start = ((), (), s32[]{:S(2)}) async-start(), calls=%async_computation.5 | async-start | bytes 8912896 | tf_op jit(solution)/shard_map/all_gather | solution.py:182
  187.1 692.8 %reduce-scatter.2.cloned.1.call-start = ((), (), s32[]{:S(2)}) async-start(), calls=%async_computation.9 | async-start | bytes 3145728 | tf_op jit(solution)/shard_map/reduce_scatter | solution.py:185
  338.5 156.9 %collective-permute-start = (bf16[2,128,4,128]{3,1,2,0:T(8,128)(2,1)S(1)}, bf16[2,128,4,128]{3,1,2,0:T(8,128)(2,1)S(1)}, u32[]{:S(2)}, u32[]{:S(2)}) collective-permute-start(bf16[2,128,4,128]{3,1,2,0:T(8,128)(2,1)S(1)} %get-tuple-element.313), channel_id=1, source_target_pairs={{0,2},{2,4},{4,6},{6,8},{8,10},{10,12},{12,14},{14,16},{16,18},{18... | collective-permute-start | bytes 786440 | tf_op jit(solution)/shard_map/ppermute | solution.py:18
  341.8 153.6 %collective-permute-start.1 = (bf16[2,128,4,128]{3,1,2,0:T(8,128)(2,1)S(1)}, bf16[2,128,4,128]{3,1,2,0:T(8,128)(2,1)S(1)}, u32[]{:S(2)}, u32[]{:S(2)}) collective-permute-start(bf16[2,128,4,128]{3,1,2,0:T(8,128)(2,1)S(1)} %get-tuple-element.314), channel_id=1, source_target_pairs={{2,0},{4,2},{6,4},{8,6},{10,8},{12,10},{14,12},{16,14},{18,16},{20... | collective-permute-start | bytes 786440 | tf_op jit(solution)/shard_map/ppermute | solution.py:19
  413.0 77.0 %copy-start.8 = (f32[256]{0:T(256)S(1)}, f32[256]{0:T(256)}, u32[]{:S(2)}) copy-start(f32[256]{0:T(256)} %copy-done.7) | copy-start | bytes 3076
  551.8 91.1 %copy-start.1 = (f32[4,256,256]{2,1,0:T(8,128)S(1)}, f32[4,256,256]{2,1,0:T(8,128)}, u32[]{:S(2)}) copy-start(f32[4,256,256]{2,1,0:T(8,128)} %convolution_multiply_fusion) | copy-start | bytes 3145732
  613.8 113.8 %copy-start.9 = (f32[256]{0:T(256)S(1)}, f32[256]{0:T(256)}, u32[]{:S(2)}) copy-start(f32[256]{0:T(256)} %copy-done.7) | copy-start | bytes 3076
  863.0 6.1 copy-start
  (2 other events, 4.1 us)
Sparse Core Ops, SparseCore 0:
  10.1 13.2 all-gather.15
  26.2 76.7 all-gather.29
  105.8 74.1 all-gather.25
  182.6 74.3 all-gather.17
  259.7 74.1 all-gather.19
  336.5 76.4 all-gather.35
  415.8 74.1 all-gather.27
  492.8 58.9 all-gather.33
  554.6 59.1 all-gather.31
  616.4 111.1 all-gather.21
  730.3 132.6 all-gather.23
  871.9 7.9 reduce-scatter.1
